TPU v7x, 32 devices: a whole 2x2x4 slice. The times are simulated.
32 devices in a mesh: fs: 4 (over y, x), tp: 8 (over z, core).
Axes of the slice: x: 2, y: 2, z: 4, core: 2. Of those that a mesh axis runs over, the one named last changes fastest.
Arguments:
- tokens: bfloat16 [1024, 2048], P('fs', 'tp'), may hold values from -60 to 60
- norm_gain: float32 [2048], P('fs'), may hold values from 0.1 to 1.9
- gate_weight: float32 [4, 2048, 4096], P(None, 'fs', 'tp'), may hold values from -0.125 to 0.125
- up_weight: float32 [4, 2048, 4096], P(None, 'fs', 'tp'), may hold values from -0.125 to 0.125
- down_weight: float32 [4, 2048, 4096], P(None, 'fs', 'tp'), may hold values from -0.125 to 0.125
- route: int32 [1024, 2], P('fs'), may hold values from 0 to 3, all different within a row; in each aligned block of 256 rows (0 to 255, 256 to 511, ...) at most 256 rows name the same one
- route_weight: float32 [1024, 2], P('fs'), may hold values from 0.2 to 1
Outputs:
- mixed: bfloat16 [1024, 2048], P('fs', 'tp')
- gate_new: bfloat16 [4, 2048, 4096], P('fs', None, 'tp')
- up_new: bfloat16 [4, 2048, 4096], P('fs', None, 'tp')
- down_new: bfloat16 [4, 2048, 4096], P('fs', None, 'tp')
Inputs may be any that keep to these rules, and one draw needn't show every extreme that they name: `route`: the 2 experts of a row differ. In each aligned block of 256 rows (the tokens of one index of fs) no expert is named by more than 256 rows, a bound that some block reaches.
All inputs are finite; a program needn't handle non-finite values.
Results may differ from a plain program's by a relative error of at most 0.024.
Values may be sent and summed in bfloat16 or wider, within the bound.
A program may use at most 64 MiB of HBM per device.

v0:
```python
import jax
import jax.numpy as jnp
from jax import lax
from jax.sharding import PartitionSpec as P

epsilon = 1e-05


def slot_table(route, block_rows, expert_count):
    pair_ids = route.reshape(-1, block_rows * route.shape[1])
    onehot = (
        pair_ids[:, :, None] == jnp.arange(expert_count, dtype=jnp.int32)[None, None, :]
    ).astype(jnp.int32)
    before = jnp.cumsum(onehot, axis=1) - onehot
    return jnp.sum(before * onehot, axis=2).reshape(route.shape)


def body(tokens, norm_gain, gate_weight, up_weight, down_weight, route, route_weight):
    experts = gate_weight.shape[0]
    tok_rows = tokens.shape[0]
    columns = tokens.shape[1]
    fs_count = lax.axis_size("fs")
    capacity = 4 * tok_rows // fs_count
    gain_col = norm_gain[None, :, None]
    gate_cast = (gate_weight * gain_col).astype(jnp.bfloat16)
    up_cast = (up_weight * gain_col).astype(jnp.bfloat16)
    down_cast = down_weight.astype(jnp.bfloat16)
    gate_new, up_new, down_new = (
        lax.all_to_all(gate_cast, "fs", split_axis=0, concat_axis=1, tiled=True),
        lax.all_to_all(up_cast, "fs", split_axis=0, concat_axis=1, tiled=True),
        lax.all_to_all(down_cast, "fs", split_axis=0, concat_axis=1, tiled=True),
    )
    slot_of = slot_table(route, tok_rows, experts)
    target = route * capacity + slot_of
    slot_lanes = jnp.arange(experts * capacity, dtype=jnp.int32)
    slot_hits = target[:, :, None] == slot_lanes[None, None, :]
    token_iota = jnp.arange(tok_rows, dtype=jnp.int32)[:, None, None]
    lane_token = jnp.sum(jnp.where(slot_hits, token_iota + 1, 0), axis=(0, 1)) - 1
    lane_token = jnp.where(lane_token < 0, tok_rows, lane_token)
    combine = jnp.sum(jnp.where(slot_hits, route_weight[:, :, None], 0.0), axis=1)
    tok_float = tokens.astype(jnp.float32)
    square_sum = lax.psum(jnp.sum(tok_float * tok_float, axis=1), "tp")
    full_width = columns * lax.axis_size("tp")
    normed = (tok_float * lax.rsqrt(square_sum / full_width + epsilon)[:, None]).astype(
        jnp.bfloat16
    )
    padded = jnp.concatenate([normed, jnp.zeros((1, columns), jnp.bfloat16)], axis=0)
    outgoing = padded[lane_token].reshape(experts, capacity, columns)
    arrived = lax.all_to_all(outgoing, "fs", split_axis=0, concat_axis=0, tiled=True).reshape(
        -1, columns
    )
    gate_local = gate_new[0]
    up_local = up_new[0]
    piece_rows = lax.all_gather(arrived, "tp", axis=1, tiled=True)
    gate_acc = jnp.dot(piece_rows, gate_local, preferred_element_type=jnp.float32)
    up_acc = jnp.dot(piece_rows, up_local, preferred_element_type=jnp.float32)
    hidden = (jax.nn.silu(gate_acc) * up_acc).astype(jnp.bfloat16)
    down_local = down_new[0]
    summed = lax.psum_scatter(
        lax.dot_general(
            down_local, hidden, (((1,), (1,)), ((), ())), preferred_element_type=jnp.float32
        ).astype(jnp.bfloat16),
        "tp",
        scatter_dimension=0,
        tiled=True,
    ).astype(jnp.float32)
    own_columns = summed.shape[0]
    outgoing_back = summed.astype(jnp.bfloat16).reshape(own_columns, fs_count, capacity)
    returned = lax.all_to_all(outgoing_back, "fs", split_axis=1, concat_axis=1, tiled=True).reshape(
        own_columns, experts * capacity
    )
    mixed = lax.dot_general(
        combine,
        returned.astype(jnp.float32),
        (((1,), (1,)), ((), ())),
        precision=lax.Precision.HIGHEST,
        preferred_element_type=jnp.float32,
    )
    return (mixed.astype(jnp.bfloat16), gate_new, up_new, down_new)


def solution(mesh):
    in_specs = (
        P("fs", "tp"),
        P("fs"),
        P(None, "fs", "tp"),
        P(None, "fs", "tp"),
        P(None, "fs", "tp"),
        P("fs", None),
        P("fs", None),
    )
    out_specs = (P("fs", "tp"), P("fs", None, "tp"), P("fs", None, "tp"), P("fs", None, "tp"))
    return jax.shard_map(body, mesh=mesh, in_specs=in_specs, out_specs=out_specs, check_vma=False)
```

profile of v0, /device:TPU:0, one launch (start us, length us, event | category | flops | bytes accessed | tf_op | source)
XLA Modules:
  0.0 224.2 jit_solution(16390866846317587679)
XLA Ops:
  7.2 0.0 all-gather.2.cloned.1.call-start
  7.2 0.8 copy.21
  8.0 0.1 eq.40
  8.2 1.2 reduce-window.6
  9.4 0.2 slice_reduce_fusion
  9.7 0.2 reduce-window.9
  9.9 0.1 broadcast.105
  10.0 0.1 reshape.192
  10.1 0.1 copy.22
  10.2 0.7 multiply_add_fusion
  10.9 0.3 select_reduce_fusion
  11.2 1.0 fusion
  12.2 18.1 %psum.7 = f32[256]{0:T(256)S(1)} all-reduce(f32[256]{0:T(256)S(1)} %fusion), channel_id=1, replica_groups=mesh['fs'=4,'tp'=8] {'tp'}, use_global_device_ids=true, to_apply=%region_5.6 | all-reduce | flops 256 | bytes 2048 | tf_op jit(solution)/shard_map/psum | solution.py:42
  30.4 1.0 fusion.1
  31.4 0.0 copy-start.1
  31.4 3.9 %gather_fusion = bf16[1024,256]{1,0:T(8,128)(2,1)S(1)} fusion(bf16[257,256]{1,0:T(8,128)(2,1)S(1)} %concatenate.3, s32[1024]{0:T(1024)S(1)} %broadcast_clamp_fusion), kind=kCustom, calls=%fused_computation | custom fusion | bytes 1052672 | tf_op jit(solution)/shard_map/gather | solution.py:48
  35.3 10.7 %all_to_all.46 = bf16[4,256,256]{2,1,0:T(8,128)(2,1)} all-to-all(bf16[4,256,256]{2,1,0:T(8,128)(2,1)S(1)} %bitcast.31), channel_id=1, replica_groups=mesh['fs'=4,'tp'=8] {'fs'}, dimensions={0} | all-to-all | bytes 1048576 | tf_op jit(solution)/shard_map/all_to_all | solution.py:49
  46.1 0.0 all-gather.2.cloned.1.call-update
  46.1 0.0 copy-done.1
  46.1 6.1 %multiply_convert_fusion = (bf16[4,512,512]{2,1,0:T(8,128)(2,1)}, bf16[4,512,512]{2,1,0:T(8,128)(2,1)S(1)}) fusion(f32[4,512,512]{2,1,0:T(8,128)} %param.10, f32[512]{0:T(512)S(1)} %copy-done.1, f32[4,512,512]{2,1,0:T(8,128)} %param.9), kind=kLoop, calls=%fused_computation.2 | loop fusion | flops 4194304 | bytes 12584960 | tf_op jit(solution)/shard_map/convert_element_type | solution.py:26
  52.3 23.8 %all_to_all.47 = bf16[4,512,512]{2,1,0:T(8,128)(2,1)S(1)} all-to-all(bf16[4,512,512]{2,1,0:T(8,128)(2,1)S(1)} %get-tuple-element.5), channel_id=1, replica_groups=mesh['fs'=4,'tp'=8] {'fs'}, dimensions={0} | all-to-all | bytes 4194304 | tf_op jit(solution)/shard_map/all_to_all | solution.py:29
  76.1 4.5 %all-to-all-start.2 = ((bf16[4,512,512]{2,1,0:T(8,128)(2,1)}), bf16[4,512,512]{2,1,0:T(8,128)(2,1)}, u32[]{:S(2)}, u32[]{:S(2)}) async-start(bf16[4,512,512]{2,1,0:T(8,128)(2,1)} %get-tuple-element.4), calls=%async_computation.2 | async-start | bytes 4194304 | tf_op jit(solution)/shard_map/all_to_all | solution.py:30
  80.6 3.8 %convert_element_type.47 = bf16[4,512,512]{2,1,0:T(8,128)(2,1)} convert(f32[4,512,512]{2,1,0:T(8,128)} %param.11) | non-fusion elementwise | flops 1048576 | bytes 6291456 | tf_op jit(solution)/shard_map/convert_element_type | solution.py:27
  84.4 16.0 %all-to-all-done.2 = bf16[4,512,512]{2,1,0:T(8,128)(2,1)} async-done(((bf16[4,512,512]{2,1,0:T(8,128)(2,1)}), bf16[4,512,512]{2,1,0:T(8,128)(2,1)}, u32[]{:S(2)}, u32[]{:S(2)}) %all-to-all-start.2) | async-done | bytes 2097184 | tf_op jit(solution)/shard_map/all_to_all | solution.py:30
  100.4 4.5 %all-to-all-start.3 = ((bf16[4,512,512]{2,1,0:T(8,128)(2,1)}), bf16[4,512,512]{2,1,0:T(8,128)(2,1)}, u32[]{:S(2)}, u32[]{:S(2)}) async-start(bf16[4,512,512]{2,1,0:T(8,128)(2,1)} %convert_element_type.47), calls=%async_computation.3 | async-start | bytes 4194304 | tf_op jit(solution)/shard_map/all_to_all | solution.py:31
  104.9 0.0 reduce-scatter.2.cloned.1.call-start
  104.9 0.0 all-gather.2.cloned.1.call-done
  104.9 5.8 %fusion.5 = f32[1024,512]{1,0:T(8,128)} fusion(bf16[1024,2048]{1,0:T(8,128)(2,1)} %all-gather.2.cloned.1.call-done, bf16[2048,512]{1,0:T(8,128)(2,1)S(1)} %bitcast.28), kind=kOutput, calls=%fused_computation.28 | convolution fusion | flops 2147483648 | bytes 8388608 | tf_op jit(solution)/shard_map/dot_general | solution.py:55
  110.8 18.5 %all-to-all-done.3 = bf16[4,512,512]{2,1,0:T(8,128)(2,1)} async-done(((bf16[4,512,512]{2,1,0:T(8,128)(2,1)}), bf16[4,512,512]{2,1,0:T(8,128)(2,1)}, u32[]{:S(2)}, u32[]{:S(2)}) %all-to-all-start.3) | async-done | bytes 2097184 | tf_op jit(solution)/shard_map/all_to_all | solution.py:31
  129.3 10.6 %convert_bitcast_fusion = bf16[2048,1024]{0,1:T(8,128)(2,1)} fusion(bf16[2048,512]{1,0:T(8,128)(2,1)} %bitcast.9, f32[1024,512]{1,0:T(8,128)} %fusion.5, bf16[1024,2048]{1,0:T(8,128)(2,1)} %all-gather.2.cloned.1.call-done, bf16[2048,512]{1,0:T(8,128)(2,1)} %bitcast.8), kind=kOutput, calls=%fused_computation.1 | convolution fusion | flops 4300210176 | bytes 14680064 | tf_op jit(solution)/shard_map/dot_general | solution.py:60
  139.9 0.0 copy-start
  139.9 0.0 reduce-scatter.2.cloned.1.call-update
  139.9 56.9 %reduce-scatter.2.cloned.1.call-done = bf16[256,1024]{0,1:T(8,128)(2,1)} async-done(((bf16[2048,1024]{0,1:T(8,128)(2,1)}), bf16[256,1024]{0,1:T(8,128)(2,1)}) %reduce-scatter.2.cloned.1.call-update) | async-done | bytes 524304 | tf_op jit(solution)/shard_map/reduce_scatter | solution.py:59
  196.8 4.1 %all-to-all-start.4 = ((bf16[256,4,256]{0,2,1:T(8,128)(2,1)}), bf16[256,4,256]{0,2,1:T(8,128)(2,1)}, u32[]{:S(2)}, u32[]{:S(2)}) async-start(bf16[256,4,256]{0,2,1:T(8,128)(2,1)} %bitcast.32), calls=%async_computation.5 | async-start | bytes 1048576 | tf_op jit(solution)/shard_map/all_to_all | solution.py:69
  201.0 0.0 copy-done
  201.0 0.3 select_reduce_fusion.1
  201.3 6.4 %all-to-all-done.4 = bf16[256,4,256]{0,2,1:T(8,128)(2,1)} async-done(((bf16[256,4,256]{0,2,1:T(8,128)(2,1)}), bf16[256,4,256]{0,2,1:T(8,128)(2,1)}, u32[]{:S(2)}, u32[]{:S(2)}) %all-to-all-start.4) | async-done | bytes 524320 | tf_op jit(solution)/shard_map/all_to_all | solution.py:69
  207.6 2.3 %convolution_convert_fusion = bf16[256,256]{1,0:T(8,128)(2,1)} fusion(f32[256,1024]{1,0:T(8,128)S(1)} %select_reduce_fusion.1, bf16[256,1024]{0,1:T(8,128)(2,1)} %bitcast.12), kind=kOutput, calls=%fused_computation.8 | convolution fusion | flops 805371904 | bytes 1703936 | tf_op jit(solution)/shard_map/dot_general | solution.py:72
  209.9 1.3 copy.26
  211.3 3.0 %copy.27 = bf16[1,2048,512]{2,1,0:T(8,128)(2,1)} copy(bf16[1,2048,512]{2,1,0:T(8,128)(2,1)} %bitcast.14) | data formatting | bytes 4194304
  214.3 3.0 %copy.28 = bf16[1,2048,512]{2,1,0:T(8,128)(2,1)} copy(bf16[1,2048,512]{2,1,0:T(8,128)(2,1)} %bitcast.15) | data formatting | bytes 4194304
  (12 shorter events, 0.1 us)
Async XLA Ops:
  7.2 97.8 %all-gather.2.cloned.1.call-start = ((), (), s32[]{:S(2)}) async-start(), calls=%async_computation.6 | async-start | bytes 4718592 | tf_op jit(solution)/shard_map/all_gather | solution.py:54
  31.4 14.7 %copy-start.1 = (f32[512]{0:T(512)S(1)}, f32[512]{0:T(512)}, u32[]{:S(2)}) copy-start(f32[512]{0:T(512)} %param.8) | copy-start | bytes 6148
  76.1 24.3 %all-to-all-start.2 = ((bf16[4,512,512]{2,1,0:T(8,128)(2,1)}), bf16[4,512,512]{2,1,0:T(8,128)(2,1)}, u32[]{:S(2)}, u32[]{:S(2)}) async-start(bf16[4,512,512]{2,1,0:T(8,128)(2,1)} %get-tuple-element.4), calls=%async_computation.2 | async-start | bytes 4194304 | tf_op jit(solution)/shard_map/all_to_all | solution.py:30
  100.4 28.9 %all-to-all-start.3 = ((bf16[4,512,512]{2,1,0:T(8,128)(2,1)}), bf16[4,512,512]{2,1,0:T(8,128)(2,1)}, u32[]{:S(2)}, u32[]{:S(2)}) async-start(bf16[4,512,512]{2,1,0:T(8,128)(2,1)} %convert_element_type.47), calls=%async_computation.3 | async-start | bytes 4194304 | tf_op jit(solution)/shard_map/all_to_all | solution.py:31
  104.9 92.0 %reduce-scatter.2.cloned.1.call-start = ((), (), s32[]{:S(2)}) async-start(), calls=%async_computation.7 | async-start | bytes 4718592 | tf_op jit(solution)/shard_map/reduce_scatter | solution.py:59
  139.9 61.1 %copy-start = (f32[256,2]{0,1:T(2,128)S(1)}, f32[256,2]{0,1:T(2,128)}, u32[]{:S(2)}) copy-start(f32[256,2]{0,1:T(2,128)} %param.13) | copy-start | bytes 6148
  196.8 10.8 %all-to-all-start.4 = ((bf16[256,4,256]{0,2,1:T(8,128)(2,1)}), bf16[256,4,256]{0,2,1:T(8,128)(2,1)}, u32[]{:S(2)}, u32[]{:S(2)}) async-start(bf16[256,4,256]{0,2,1:T(8,128)(2,1)} %bitcast.32), calls=%async_computation.5 | async-start | bytes 1048576 | tf_op jit(solution)/shard_map/all_to_all | solution.py:69
Sparse Core Ops, SparseCore 0:
  46.2 44.4 all-gather.1
  140.0 56.7 reduce-scatter.1
where the time goes:
time: 225 us; the launch traced here: 224 us
  waiting for transfers between devices  97.9 us (44%)
  blocking collectives  52.7 us (23%)
  matrix products  18.7 us (8%)
  other arithmetic  14.6 us (6%)
  between operations  14.2 us (6%)
  starting transfers between devices  13.2 us (6%)
  local copies, waits for them, and re-layouts  12.9 us (6%)
    reduce_scatter x1, waiting for transfers between devices, body(): lax.psum_scatter(lax.dot_general(down_local, hidden, (((1,), (1,)), ((),...  56.9 us
    all_to_all x1, blocking collectives, body(): lax.all_to_all(gate_cast, 'fs', split_axis=0, concat_axis=1, tiled=True)  23.8 us
    all_to_all x1, waiting for transfers between devices, body(): lax.all_to_all(down_cast, 'fs', split_axis=0, concat_axis=1, tiled=True)  18.5 us
    psum x1, blocking collectives, body(): square_sum = lax.psum(jnp.sum(tok_float * tok_float, axis=1), 'tp')  18.1 us
    all_to_all x1, waiting for transfers between devices, body(): lax.all_to_all(up_cast, 'fs', split_axis=0, concat_axis=1, tiled=True)  16 us
    all_to_all x1, blocking collectives, body(): lax.all_to_all(outgoing, 'fs', split_axis=0, concat_axis=0, tiled=True)  10.7 us
    dot_general x1, matrix products, body(): lax.dot_general(down_local, hidden, (((1,), (1,)), ((), ())), preferred_e...  10.6 us
    unnamed x8, local copies, waits for them, and re-layouts  8.23 us
  transfers between devices with their start and end apart: 5, of which 4 were waited for; matrix products, arithmetic and copies ran while one was open for 7% of the time, Pallas kernels for 0%

commit v1 on v0

--- a/solution.py
+++ b/solution.py
@@ -1,6 +1,10 @@
+import functools
+
 import jax
 import jax.numpy as jnp
 from jax import lax
+from jax.experimental import pallas as pl
+from jax.experimental.pallas import tpu as pltpu
 from jax.sharding import PartitionSpec as P
 
 epsilon = 1e-05
@@ -15,7 +19,7 @@
     return jnp.sum(before * onehot, axis=2).reshape(route.shape)
 
 
-def body(tokens, norm_gain, gate_weight, up_weight, down_weight, route, route_weight):
+def slotted_body(tokens, norm_gain, gate_weight, up_weight, down_weight, route, route_weight):
     experts = gate_weight.shape[0]
     tok_rows = tokens.shape[0]
     columns = tokens.shape[1]
@@ -79,6 +83,429 @@
     return (mixed.astype(jnp.bfloat16), gate_new, up_new, down_new)
 
 
+MESH = pl.DeviceIdType.MESH
+STAGES = 2
+ROW_TILE = 256
+
+
+def flip(index, distance):
+    bit = 1
+    while bit <= distance:
+        if distance & bit:
+            index = index + bit - 2 * bit * ((index // bit) % 2)
+        bit *= 2
+    return index
+
+
+def rows_of(index, size):
+    return pl.ds(pl.multiple_of(index * size, size), size)
+
+
+def moe_kernel(
+    fs,
+    tp,
+    tokens,
+    gain,
+    gate,
+    up,
+    down,
+    route,
+    route_weight,
+    mixed,
+    gate_out,
+    up_out,
+    down_out,
+    loaded,
+    staged,
+    w_gate,
+    w_up,
+    w_down,
+    tok_raw,
+    tok_norm,
+    hidden,
+    pair_own,
+    pair_out,
+    pair_in,
+    z_out,
+    z_in,
+    back_out,
+    back_in,
+    load_sem,
+    tok_local,
+    tf_s,
+    tf_r,
+    tz_s,
+    tz_r,
+    tw_s,
+    tw_r,
+    w_s,
+    w_r,
+    dn_s,
+    dn_r,
+    pr_s,
+    pr_r,
+    z_s,
+    z_r,
+    bk_s,
+    bk_r,
+    out_sem,
+):
+    chips = tp // 2
+    f = lax.axis_index("fs")
+    t = lax.axis_index("tp")
+    z, core = t // 2, t % 2
+    sibling = flip(t, 1)
+    block, width = tokens.shape
+    depth, units = gate.shape[1], gate.shape[2]
+    sub = width // STAGES
+    total_rows = fs * block
+    away = [fs - 1] + list(range(1, fs - 1))
+    sources, finals = (gate, up, down), (w_gate, w_up, w_down)
+
+    loads = {}
+    for p in range(3):
+        for d in away + [0]:
+            loads[p, d] = pltpu.make_async_copy(
+                sources[p].at[flip(f, d)], loaded.at[p, d], load_sem.at[p, d]
+            )
+            loads[p, d].start()
+    own_tok = pltpu.make_async_copy(tokens, tok_raw.at[t, rows_of(f, block)], tok_local)
+    own_tok.start()
+
+    barrier = pltpu.get_barrier_semaphore()
+    for d in range(1, fs):
+        pl.semaphore_signal(barrier, inc=1, device_id={"fs": flip(f, d)}, device_id_type=MESH)
+    for d in range(1, tp):
+        pl.semaphore_signal(barrier, inc=1, device_id={"tp": flip(t, d)}, device_id_type=MESH)
+    pl.semaphore_wait(barrier, fs + tp - 2)
+
+    sent = []
+
+    def send(src, dst, s_sem, r_sem, **device):
+        copy = pltpu.make_async_remote_copy(
+            src_ref=src,
+            dst_ref=dst,
+            send_sem=s_sem,
+            recv_sem=r_sem,
+            device_id=device,
+            device_id_type=MESH,
+        )
+        copy.start()
+        sent.append(copy)
+        return copy
+
+    tok_fs = [
+        send(tokens, tok_raw.at[t, rows_of(f, block)], tf_s.at[d], tf_r.at[d], fs=flip(f, d))
+        for d in range(1, fs)
+    ]
+
+    def cast(p, d):
+        loads[p, d].wait()
+        tile = 64
+
+        @pl.loop(0, depth // tile)
+        def _(i):
+            rows = rows_of(i, tile)
+            value = loaded[p, d, rows, :]
+            if p < 2:
+                value = value * gain[rows, :]
+            value = value.astype(jnp.bfloat16)
+            if d:
+                staged[p, d - 1, rows, :] = value
+            else:
+                finals[p][pl.ds(pl.multiple_of(f * depth + i * tile, tile), tile), :] = value
+
+    arrive = {}
+
+    def ship(p, d):
+        cast(p, d)
+        arrive[p, d] = send(
+            staged.at[p, d - 1],
+            finals[p].at[rows_of(f, depth)],
+            w_s.at[p, d],
+            w_r.at[p, d],
+            fs=flip(f, d),
+        )
+
+    for d in away:
+        ship(0, d)
+
+    own_tok.wait()
+    for copy in tok_fs:
+        copy.wait_recv()
+    tok_z = {
+        d: send(tok_raw.at[t], tok_raw.at[t], tz_s.at[d], tz_r.at[d], tp=flip(t, 2 * d))
+        for d in range(1, chips)
+    }
+    tok_pair = send(tok_raw.at[t], tok_raw.at[t], tz_s.at[0], tz_r.at[0], tp=sibling)
+
+    for d in away:
+        ship(1, d)
+    for d in away:
+        cast(2, d)
+    for u in range(STAGES):
+        for d in away:
+            for c in range(2):
+                arrive[2, u, d, c] = send(
+                    staged.at[2, d - 1, pl.ds(c * width + u * sub, sub)],
+                    w_down.at[
+                        pl.ds(pl.multiple_of(f * depth + (c * width + u * sub), sub), sub)
+                    ],
+                    dn_s.at[u, d, c],
+                    dn_r.at[u, d, c],
+                    fs=flip(f, d),
+                )
+    for p in range(3):
+        cast(p, 0)
+
+    forwards = []
+    for d in range(1, chips):
+        tok_z[d].wait_recv()
+        there = flip(t, 2 * d)
+        forwards.append(
+            send(tok_raw.at[there], tok_raw.at[there], tw_s.at[d], tw_r.at[d], tp=sibling)
+        )
+    tok_pair.wait_recv()
+    for copy in forwards:
+        copy.wait_recv()
+
+    @pl.loop(0, total_rows // 64)
+    def _(i):
+        rows = rows_of(i, 64)
+        squares = jnp.zeros((64, 1), jnp.float32)
+        for k in range(tp):
+            value = tok_raw[k, rows, :].astype(jnp.float32)
+            squares = squares + jnp.sum(value * value, axis=1, keepdims=True)
+        scale = lax.rsqrt(squares / (width * tp) + epsilon)
+        for k in range(tp):
+            value = tok_raw[k, rows, :].astype(jnp.float32)
+            tok_norm[rows, k * width : (k + 1) * width] = (value * scale).astype(jnp.bfloat16)
+
+    for p in range(2):
+        for d in away:
+            arrive[p, d].wait_recv()
+    outs = [
+        pltpu.make_async_copy(w_gate, gate_out, out_sem.at[0]),
+        pltpu.make_async_copy(w_up, up_out, out_sem.at[1]),
+        pltpu.make_async_copy(w_down, down_out, out_sem.at[2]),
+    ]
+    outs[0].start()
+    outs[1].start()
+
+    @pl.loop(0, total_rows // ROW_TILE)
+    def _(i):
+        rows = rows_of(i, ROW_TILE)
+        value = tok_norm[rows, :]
+        gate_acc = jnp.dot(value, w_gate[...], preferred_element_type=jnp.float32)
+        up_acc = jnp.dot(value, w_up[...], preferred_element_type=jnp.float32)
+        hidden[rows, :] = (jax.nn.silu(gate_acc) * up_acc).astype(jnp.bfloat16)
+
+    def product(u, d):
+        s = flip(f, d)
+        if d:
+            for c in range(2):
+                arrive[2, u, d, c].wait_recv()
+
+        def weights(c):
+            start = pl.multiple_of(s * depth + c * width + u * sub, sub)
+            return w_down[pl.ds(start, sub), :]
+
+        @pl.loop(0, total_rows // ROW_TILE)
+        def _(i):
+            rows = rows_of(i, ROW_TILE)
+            value = hidden[rows, :]
+            dims = (((1,), (1,)), ((), ()))
+            pair_own[u, d, rows, :] = lax.dot_general(
+                value, weights(core), dims, preferred_element_type=jnp.float32
+            )
+            pair_out[u, d, rows, :] = lax.dot_general(
+                value, weights(1 - core), dims, preferred_element_type=jnp.float32
+            ).astype(jnp.bfloat16)
+
+        return send(
+            pair_out.at[u, d], pair_in.at[u, d], pr_s.at[u, d], pr_r.at[u, d], tp=sibling
+        )
+
+    z_sends = []
+
+    def pass_on(u, d, copy):
+        s = flip(f, d)
+        copy.wait_recv()
+
+        def total(rows):
+            value = pair_own[u, d, rows, :] + pair_in[u, d, rows, :].astype(jnp.float32)
+            return value.astype(jnp.bfloat16)
+
+        @pl.loop(0, total_rows // ROW_TILE)
+        def _(i):
+            rows = rows_of(i, ROW_TILE)
+            z_out[u, d, rows, :] = total(rows)
+
+        across = pltpu.make_async_remote_copy(
+            src_ref=z_out.at[u, d],
+            dst_ref=z_in.at[u, z],
+            send_sem=z_s.at[u, d],
+            recv_sem=z_r.at[u, z],
+            device_id={"tp": s * 2 + core},
+            device_id_type=MESH,
+        )
+
+        @pl.when(s != z)
+        def _():
+            across.start()
+
+        @pl.when(s == z)
+        def _():
+            @pl.loop(0, total_rows // ROW_TILE)
+            def _(i):
+                rows = rows_of(i, ROW_TILE)
+                z_in[u, z, rows, :] = z_out[u, d, rows, :]
+
+        z_sends.append((s, across))
+
+    returns = []
+
+    def finish(u):
+        for d in range(1, chips):
+            there = flip(z, d)
+            pltpu.make_async_remote_copy(
+                src_ref=z_out.at[u, d],
+                dst_ref=z_in.at[u, there],
+                send_sem=z_s.at[u, d],
+                recv_sem=z_r.at[u, there],
+                device_id={"tp": there * 2 + core},
+                device_id_type=MESH,
+            ).wait_recv()
+        for d in away + [0]:
+            b = flip(f, d)
+            rows = rows_of(b, block)
+            value = jnp.zeros((block, sub), jnp.float32)
+            for k in range(chips):
+                value = value + z_in[u, k, rows, :].astype(jnp.float32)
+            value = value.astype(jnp.bfloat16)
+            if d:
+                back_out[u, d] = value
+                returns.append(
+                    send(
+                        back_out.at[u, d],
+                        back_in.at[u, f],
+                        bk_s.at[u, d],
+                        bk_r.at[u, d],
+                        fs=b,
+                    )
+                )
+            else:
+                back_in[u, f] = value
+
+    items = [(u, 0) for u in range(STAGES)]
+    items += [(u, d) for u in range(STAGES) for d in list(range(1, fs - 1)) + [fs - 1]]
+    waiting = None
+    for item in items:
+        copy = product(*item)
+        if waiting is not None:
+            pass_on(*waiting)
+        waiting = item + (copy,)
+    outs[2].start()
+    pass_on(*waiting)
+    for u in range(STAGES):
+        finish(u)
+    for copy in returns:
+        copy.wait_recv()
+    for u in range(STAGES):
+        value = jnp.zeros((block, sub), jnp.float32)
+        for e in range(fs):
+            share = jnp.zeros((block, 1), jnp.float32)
+            for k in range(route.shape[1]):
+                share = share + jnp.where(
+                    route[:, k : k + 1] == e, route_weight[:, k : k + 1], 0.0
+                )
+            value = value + share * back_in[u, e].astype(jnp.float32)
+        mixed[:, u * sub : (u + 1) * sub] = value.astype(jnp.bfloat16)
+
+    for copy in sent:
+        copy.wait_send()
+    for s, across in z_sends:
+
+        @pl.when(s != z)
+        def _():
+            across.wait_send()
+
+    for copy in outs:
+        copy.wait()
+
+
+def dense_body(tokens, norm_gain, gate_weight, up_weight, down_weight, route, route_weight):
+    fs, tp = lax.axis_size("fs"), lax.axis_size("tp")
+    block, width = tokens.shape
+    experts, depth, units = gate_weight.shape
+    rows, full, sub = fs * block, tp * width, width // STAGES
+    whole = pl.BlockSpec(memory_space=pltpu.VMEM)
+    far = pl.BlockSpec(memory_space=pl.ANY)
+    narrow, dma = jnp.bfloat16, pltpu.SemaphoreType.DMA
+    weight = jax.ShapeDtypeStruct((full, units), narrow)
+    mixed, gate_new, up_new, down_new = pl.pallas_call(
+        functools.partial(moe_kernel, fs, tp),
+        out_shape=(jax.ShapeDtypeStruct((block, width), narrow), weight, weight, weight),
+        in_specs=[whole, whole, far, far, far, whole, whole],
+        out_specs=(whole, far, far, far),
+        scratch_shapes=[
+            pltpu.VMEM((3, experts, depth, units), jnp.float32),
+            pltpu.VMEM((3, fs - 1, depth, units), narrow),
+            pltpu.VMEM((full, units), narrow),
+            pltpu.VMEM((full, units), narrow),
+            pltpu.VMEM((full, units), narrow),
+            pltpu.VMEM((tp, rows, width), narrow),
+            pltpu.VMEM((rows, full), narrow),
+            pltpu.VMEM((rows, units), narrow),
+            pltpu.VMEM((STAGES, fs, rows, sub), jnp.float32),
+            pltpu.VMEM((STAGES, fs, rows, sub), narrow),
+            pltpu.VMEM((STAGES, fs, rows, sub), narrow),
+            pltpu.VMEM((STAGES, fs, rows, sub), narrow),
+            pltpu.VMEM((STAGES, tp // 2, rows, sub), narrow),
+            pltpu.VMEM((STAGES, fs, block, sub), narrow),
+            pltpu.VMEM((STAGES, fs, block, sub), narrow),
+            dma((3, experts)),
+            dma,
+            dma((fs,)),
+            dma((fs,)),
+            dma((tp // 2,)),
+            dma((tp // 2,)),
+            dma((tp // 2,)),
+            dma((tp // 2,)),
+            dma((2, fs)),
+            dma((2, fs)),
+            dma((STAGES, fs, 2)),
+            dma((STAGES, fs, 2)),
+            dma((STAGES, fs)),
+            dma((STAGES, fs)),
+            dma((STAGES, fs)),
+            dma((STAGES, tp // 2)),
+            dma((STAGES, fs)),
+            dma((STAGES, fs)),
+            dma((3,)),
+        ],
+        compiler_params=pltpu.CompilerParams(
+            collective_id=0, has_side_effects=True, vmem_limit_bytes=64000 * 1024
+        ),
+    )(tokens, norm_gain[:, None], gate_weight, up_weight, down_weight, route, route_weight)
+    return mixed, gate_new[None], up_new[None], down_new[None]
+
+
+def body(tokens, norm_gain, gate_weight, up_weight, down_weight, route, route_weight):
+    fs, tp = lax.axis_size("fs"), lax.axis_size("tp")
+    fits = (
+        fs == 4
+        and tp == 2 * fs
+        and gate_weight.shape[0] == fs
+        and tokens.shape[1] % (128 * STAGES) == 0
+        and tokens.shape[0] % 64 == 0
+        and gate_weight.shape[1] == 2 * tokens.shape[1]
+        and tokens.shape[0] * fs * tokens.shape[1] * tp <= 1024 * 2048
+    )
+    chosen = dense_body if fits else slotted_body
+    return chosen(tokens, norm_gain, gate_weight, up_weight, down_weight, route, route_weight)
+
+
 def solution(mesh):
     in_specs = (
         P("fs", "tp"),

time: 225 us -> 146 us (0.65)
  Pallas kernels: 0 us -> 132 us
  waiting for transfers between devices: 97.9 us -> 0 us
  blocking collectives: 52.7 us -> 0 us
  matrix products: 18.7 us -> 0 us
  other arithmetic: 14.6 us -> 0 us
  between operations: 14.2 us -> 0.64 us
  starting transfers between devices: 13.2 us -> 0 us
    pallas_call x0 -> x1, Pallas kernels: none -> 132 us  [dense_body(): pl.pallas_call(functools.partial(moe_kernel, fs, tp), out_shape=(jax.Shap...]
    reduce_scatter x1 -> x0, waiting for transfers between devices: 56.9 us -> none  [body(): lax.psum_scatter(lax.dot_general(down_local, hidden, (((1,), (1,)), ((),...]
    all_to_all x3 -> x0, waiting for transfers between devices: 40.9 us -> none  [the longest x1 18.5 us: body(): lax.all_to_all(down_cast, 'fs', split_axis=0, concat_axis=1, tiled=True)]
    all_to_all x2 -> x0, blocking collectives: 34.6 us -> none  [the longest x1 23.8 us: body(): lax.all_to_all(gate_cast, 'fs', split_axis=0, concat_axis=1, tiled=True)]
    dot_general x3 -> x0, matrix products: 18.7 us -> none  [the longest x1 10.6 us: body(): lax.dot_general(down_local, hidden, (((1,), (1,)), ((), ())), preferred_e...]
    psum x1 -> x0, blocking collectives: 18.1 us -> none  [body(): square_sum = lax.psum(jnp.sum(tok_float * tok_float, axis=1), 'tp')]
    all_to_all x3 -> x0, starting transfers between devices: 13.1 us -> none  [the longest x1 4.5 us: body(): lax.all_to_all(up_cast, 'fs', split_axis=0, concat_axis=1, tiled=True)]
    convert_element_type x3 -> x0, other arithmetic: 10.9 us -> none  [the longest x1 6.12 us: body(): up_cast = (up_weight * gain_col).astype(jnp.bfloat16)]
  transfers between devices with their start and end apart: 5 -> 0, of which waited for: 4 -> 0; matrix products, arithmetic and copies ran while one was open for 7% -> 0% of each run, Pallas kernels for 0% -> 0%
where the time goes in v1:
time: 146 us
  Pallas kernels  132 us (90%)
  local copies, waits for them, and re-layouts  12.9 us (9%)
    pallas_call x1, Pallas kernels, dense_body(): pl.pallas_call(functools.partial(moe_kernel, fs, tp), out_shape=(jax.Shap...  132 us
    unnamed x10, local copies, waits for them, and re-layouts  11.4 us

profile of v1, /device:TPU:0, one launch (start us, length us, event | category | flops | bytes accessed | tf_op | source)
XLA Modules:
  0.0 145.5 jit_solution(1667627477457795747)
XLA Ops:
  0.6 1.5 %copy.14.route = s32[256,2]{1,0:T(8,128)} copy(s32[256,2]{0,1:T(2,128)} %param.12) | data formatting | bytes 4096 | tf_op args[5]
  2.1 1.5 %copy.15.route_weight = f32[256,2]{1,0:T(8,128)} copy(f32[256,2]{0,1:T(2,128)} %param.13) | data formatting | bytes 4096 | tf_op args[6]
  3.6 1.5 %copy.13.gain = f32[512,1]{1,0:T(8,128)} copy(f32[512,1]{0,1:T(1,128)} %bitcast.7) | data formatting | bytes 4096 | tf_op jit(solution)/shard_map/broadcast_in_dim | solution.py:490
  5.1 132.0 %shard_map.102 = (bf16[256,256]{1,0:T(8,128)(2,1)}, bf16[2048,512]{1,0:T(8,128)(2,1)}, bf16[2048,512]{1,0:T(8,128)(2,1)}, bf16[2048,512]{1,0:T(8,128)(2,1)}) custom-call(bf16[256,256]{1,0:T(8,128)(2,1)} %tokens.1, f32[512,1]{1,0:T(8,128)} %copy.13.gain, f32[4,512,512]{2,1,0:T(8,128)} %gate.1, f32[4,512,512]{2,1,0:T(8,128)} %up.1, f32[4,512,512]{2,1,0:T(8,128)} %down.1, ...), custom_call_target="tpu_custom_call" | custom-call | tf_op jit(solution)/shard_map/pallas_call | solution.py:446
  137.1 1.6 %copy.20 = bf16[256,256]{1,0:T(8,128)(2,1)} copy(bf16[256,256]{1,0:T(8,128)(2,1)} %get-tuple-element.16) | data formatting | bytes 262144
  138.7 0.0 copy-start.1
  138.7 3.2 %copy.21 = bf16[1,2048,512]{2,1,0:T(8,128)(2,1)} copy(bf16[1,2048,512]{2,1,0:T(8,128)(2,1)} %bitcast.6) | data formatting | bytes 4194304
  141.9 0.0 copy-done.1
  141.9 0.0 copy-start
  141.9 1.3 copy.22
  143.2 1.0 copy-done
  144.2 1.3 copy.23
Async XLA Ops:
  138.7 3.2 %copy-start.1 = (bf16[2048,512]{1,0:T(8,128)(2,1)S(1)}, bf16[2048,512]{1,0:T(8,128)(2,1)}, u32[]{:S(2)}) copy-start(bf16[2048,512]{1,0:T(8,128)(2,1)} %get-tuple-element.10) | copy-start | bytes 6291460
  141.9 2.3 %copy-start = (bf16[2048,512]{1,0:T(8,128)(2,1)S(1)}, bf16[2048,512]{1,0:T(8,128)(2,1)}, u32[]{:S(2)}) copy-start(bf16[2048,512]{1,0:T(8,128)(2,1)} %get-tuple-element.11) | copy-start | bytes 6291460

commit v2 on v1

--- a/solution.py
+++ b/solution.py
@@ -130,6 +130,7 @@
     z_in,
     back_out,
     back_in,
+    gain_col,
     load_sem,
     tok_local,
     tf_s,
@@ -162,6 +163,11 @@
     away = [fs - 1] + list(range(1, fs - 1))
     sources, finals = (gate, up, down), (w_gate, w_up, w_down)
 
+    barrier = pltpu.get_barrier_semaphore()
+    for d in range(1, fs):
+        pl.semaphore_signal(barrier, inc=1, device_id={"fs": flip(f, d)}, device_id_type=MESH)
+    for d in range(1, tp):
+        pl.semaphore_signal(barrier, inc=1, device_id={"tp": flip(t, d)}, device_id_type=MESH)
     loads = {}
     for p in range(3):
         for d in away + [0]:
@@ -172,11 +178,7 @@
     own_tok = pltpu.make_async_copy(tokens, tok_raw.at[t, rows_of(f, block)], tok_local)
     own_tok.start()
 
-    barrier = pltpu.get_barrier_semaphore()
-    for d in range(1, fs):
-        pl.semaphore_signal(barrier, inc=1, device_id={"fs": flip(f, d)}, device_id_type=MESH)
-    for d in range(1, tp):
-        pl.semaphore_signal(barrier, inc=1, device_id={"tp": flip(t, d)}, device_id_type=MESH)
+    gain_col[...] = jnp.broadcast_to(gain[...], (128, depth)).T
     pl.semaphore_wait(barrier, fs + tp - 2)
 
     sent = []
@@ -196,7 +198,7 @@
 
     tok_fs = [
         send(tokens, tok_raw.at[t, rows_of(f, block)], tf_s.at[d], tf_r.at[d], fs=flip(f, d))
-        for d in range(1, fs)
+        for d in away
     ]
 
     def cast(p, d):
@@ -208,7 +210,7 @@
             rows = rows_of(i, tile)
             value = loaded[p, d, rows, :]
             if p < 2:
-                value = value * gain[rows, :]
+                value = value * gain_col[rows, 0:1]
             value = value.astype(jnp.bfloat16)
             if d:
                 staged[p, d - 1, rows, :] = value
@@ -414,11 +416,12 @@
     for u in range(STAGES):
         value = jnp.zeros((block, sub), jnp.float32)
         for e in range(fs):
-            share = jnp.zeros((block, 1), jnp.float32)
-            for k in range(route.shape[1]):
+            share = jnp.zeros((1, block), jnp.float32)
+            for k in range(route.shape[0]):
                 share = share + jnp.where(
-                    route[:, k : k + 1] == e, route_weight[:, k : k + 1], 0.0
+                    route[k : k + 1, :] == e, route_weight[k : k + 1, :], 0.0
                 )
+            share = jnp.broadcast_to(share, (sub, block)).T
             value = value + share * back_in[u, e].astype(jnp.float32)
         mixed[:, u * sub : (u + 1) * sub] = value.astype(jnp.bfloat16)
 
@@ -464,6 +467,7 @@
             pltpu.VMEM((STAGES, tp // 2, rows, sub), narrow),
             pltpu.VMEM((STAGES, fs, block, sub), narrow),
             pltpu.VMEM((STAGES, fs, block, sub), narrow),
+            pltpu.VMEM((depth, 128), jnp.float32),
             dma((3, experts)),
             dma,
             dma((fs,)),
@@ -487,7 +491,7 @@
         compiler_params=pltpu.CompilerParams(
             collective_id=0, has_side_effects=True, vmem_limit_bytes=64000 * 1024
         ),
-    )(tokens, norm_gain[:, None], gate_weight, up_weight, down_weight, route, route_weight)
+    )(tokens, norm_gain[None, :], gate_weight, up_weight, down_weight, route.T, route_weight.T)
     return mixed, gate_new[None], up_new[None], down_new[None]
 
 

time: 146 us -> 140 us (0.959)
  local copies, waits for them, and re-layouts: 12.9 us -> 8.43 us
    unnamed x10 -> x8, local copies, waits for them, and re-layouts: 11.4 us -> 8.43 us
    broadcast_in_dim x1 -> x0, local copies, waits for them, and re-layouts: 1.53 us -> none  [dense_body(): norm_gain[:, None]]
where the time goes in v2:
time: 140 us
  Pallas kernels  131 us (94%)
  local copies, waits for them, and re-layouts  8.43 us (6%)
    pallas_call x1, Pallas kernels, dense_body(): pl.pallas_call(functools.partial(moe_kernel, fs, tp), out_shape=(jax.Shap...  131 us
    unnamed x8, local copies, waits for them, and re-layouts  8.43 us

profile of v2, /device:TPU:0, one launch (start us, length us, event | category | flops | bytes accessed | tf_op | source)
XLA Modules:
  0.0 140.0 jit_solution(9266625817029027459)
XLA Ops:
  0.6 130.9 %shard_map.102 = (bf16[256,256]{1,0:T(8,128)(2,1)}, bf16[2048,512]{1,0:T(8,128)(2,1)}, bf16[2048,512]{1,0:T(8,128)(2,1)}, bf16[2048,512]{1,0:T(8,128)(2,1)}) custom-call(bf16[256,256]{1,0:T(8,128)(2,1)} %tokens.1, f32[1,512]{1,0:T(1,128)} %bitcast.9, f32[4,512,512]{2,1,0:T(8,128)} %gate.1, f32[4,512,512]{2,1,0:T(8,128)} %up.1, f32[4,512,512]{2,1,0:T(8,128)} %down.1, ...), custom_call_target="tpu_custom_call" | custom-call | tf_op jit(solution)/shard_map/pallas_call | solution.py:449
  131.5 1.6 %copy.15 = bf16[256,256]{1,0:T(8,128)(2,1)} copy(bf16[256,256]{1,0:T(8,128)(2,1)} %get-tuple-element.16) | data formatting | bytes 262144
  133.1 0.0 copy-start.1
  133.1 3.2 %copy.16 = bf16[1,2048,512]{2,1,0:T(8,128)(2,1)} copy(bf16[1,2048,512]{2,1,0:T(8,128)(2,1)} %bitcast.8) | data formatting | bytes 4194304
  136.3 0.0 copy-done.1
  136.3 0.0 copy-start
  136.3 1.3 copy.17
  137.6 1.0 copy-done
  138.7 1.3 copy.18
Async XLA Ops:
  133.1 3.2 %copy-start.1 = (bf16[2048,512]{1,0:T(8,128)(2,1)S(1)}, bf16[2048,512]{1,0:T(8,128)(2,1)}, u32[]{:S(2)}) copy-start(bf16[2048,512]{1,0:T(8,128)(2,1)} %get-tuple-element.10) | copy-start | bytes 6291460
  136.3 2.3 %copy-start = (bf16[2048,512]{1,0:T(8,128)(2,1)S(1)}, bf16[2048,512]{1,0:T(8,128)(2,1)}, u32[]{:S(2)}) copy-start(bf16[2048,512]{1,0:T(8,128)(2,1)} %get-tuple-element.11) | copy-start | bytes 6291460
